TPU v7x, 32 devices: a whole 2x2x4 slice. The times are simulated.
32 devices in a mesh: fs: 4 (over y, x), tp: 8 (over z, core).
Axes of the slice: x: 2, y: 2, z: 4, core: 2. Of those that a mesh axis runs over, the one named last changes fastest.
Arguments:
- stream_in: bfloat16 [4096, 4096], P(('fs', 'tp')), may hold values from -6 to 6
- mixer_out: bfloat16 [4096, 4096], P(('fs', 'tp')), may hold values from -6 to 6
- mix_gain: float32 [4096], replicated, may hold values from 0.1 to 1.9
- pre_gain: float32 [4096], replicated, may hold values from 0.1 to 1.9
- gate_weight: float32 [4096, 6144], P('fs', 'tp'), may hold values from -0.09375 to 0.09375
- up_weight: float32 [4096, 6144], P('fs', 'tp'), may hold values from -0.09375 to 0.09375
- gate_scale: float32 [6144], P('tp'), may hold values from 0.5 to 2
- up_scale: float32 [6144], P('tp'), may hold values from 0.5 to 2
Outputs:
- hidden: bfloat16 [4096, 6144], P('fs', 'tp')
- stream: bfloat16 [4096, 4096], P(('fs', 'tp'))
All inputs are finite; a program needn't handle non-finite values.
Results may differ from a plain program's by a relative error of at most 0.0082.
Values may be sent and summed in bfloat16 or wider, within the bound.
No kernel may reach another device: no remote copies, remote signals or barrier semaphores. Data moves between devices by JAX's collectives and lax.ppermute only.
A program may use at most 128 MiB of HBM per device.

v0:
```python
import jax
import jax.numpy as jnp
from jax import lax
from jax.sharding import PartitionSpec as P

epsilon = 1e-06


def rms_scaled(values, gain):
    return values * lax.rsqrt(jnp.mean(values * values, axis=-1, keepdims=True) + epsilon) * gain


def on_device(
    stream_in, mixer_out, mix_gain, pre_gain, gate_weight, up_weight, gate_scale, up_scale
):
    mixed = stream_in.astype(jnp.float32) + rms_scaled(mixer_out.astype(jnp.float32), mix_gain)
    stream = mixed.astype(jnp.bfloat16)
    normed = rms_scaled(stream.astype(jnp.float32), pre_gain).astype(jnp.bfloat16)
    gate_cast = gate_weight.astype(jnp.bfloat16)
    up_cast = up_weight.astype(jnp.bfloat16)
    gate_full, up_full = (
        lax.all_gather(gate_cast, "fs", axis=0, tiled=True),
        lax.all_gather(up_cast, "fs", axis=0, tiled=True),
    )
    piece = lax.all_gather(normed, "tp", axis=0, tiled=True)
    gate = jnp.dot(piece, gate_full, preferred_element_type=jnp.float32) * gate_scale
    up = jnp.dot(piece, up_full, preferred_element_type=jnp.float32) * up_scale
    hidden = (jax.nn.silu(gate) * up).astype(jnp.bfloat16)
    return (hidden, stream)


def solution(mesh):
    return jax.shard_map(
        on_device,
        mesh=mesh,
        in_specs=(
            P(("fs", "tp"), None),
            P(("fs", "tp"), None),
            P(),
            P(),
            P("fs", "tp"),
            P("fs", "tp"),
            P("tp"),
            P("tp"),
        ),
        out_specs=(P("fs", "tp"), P(("fs", "tp"), None)),
        check_vma=False,
    )
```

profile of v0, /device:TPU:0, one launch (start us, length us, event | category | flops | bytes accessed | tf_op | source)
XLA Modules:
  0.0 256.1 jit_solution(6884719773406794379)
XLA Ops:
  7.2 0.0 copy-start.1
  7.2 0.0 copy-start.3
  7.2 0.0 copy-start.2
  7.2 0.0 all-gather.6.cloned.1.call-start
  7.2 3.3 %convert_element_type.29 = bf16[1024,768]{1,0:T(8,128)(2,1)} convert(f32[1024,768]{1,0:T(8,128)} %param.12) | non-fusion elementwise | flops 786432 | bytes 4718592 | tf_op jit(solution)/shard_map/convert_element_type | solution.py:19
  10.6 0.0 copy-start.4
  10.6 0.0 all-gather.6.cloned.1.call-update
  10.6 0.0 all-gather.4.cloned.1.call-start
  10.6 0.0 copy-done.1
  10.6 0.3 fusion
  10.9 0.0 copy-done.3
  11.0 0.0 copy-done.2
  11.0 0.7 fusion.4
  11.7 0.0 copy-start
  11.7 0.0 copy-done.4
  11.7 1.3 fusion.6
  13.1 0.0 all-gather.4.cloned.1.call-update
  13.1 0.0 all-gather.8.cloned.1.call-start
  13.2 3.2 %convert_element_type.30 = bf16[1024,768]{1,0:T(8,128)(2,1)} convert(f32[1024,768]{1,0:T(8,128)} %param.13) | non-fusion elementwise | flops 786432 | bytes 4718592 | tf_op jit(solution)/shard_map/convert_element_type | solution.py:20
  16.4 0.0 copy-done
  16.4 0.0 all-gather.8.cloned.1.call-update
  16.4 0.0 copy-start.5
  16.4 0.0 copy-start.6
  16.4 67.1 %all-gather.6.cloned.1.call-done = bf16[4096,768]{1,0:T(8,128)(2,1)} async-done(((bf16[1024,768]{1,0:T(8,128)(2,1)}), bf16[4096,768]{1,0:T(8,128)(2,1)}) %all-gather.6.cloned.1.call-update) | async-done | bytes 6291472 | tf_op jit(solution)/shard_map/all_gather | solution.py:22
  83.5 83.7 %all-gather.4.cloned.1.call-done = bf16[1024,4096]{1,0:T(8,128)(2,1)} async-done(((bf16[128,4096]{1,0:T(8,128)(2,1)}), bf16[1024,4096]{1,0:T(8,128)(2,1)}) %all-gather.4.cloned.1.call-update) | async-done | bytes 8388624 | tf_op jit(solution)/shard_map/all_gather | solution.py:25
  167.2 10.9 %fusion.8 = f32[1024,768]{1,0:T(8,128)S(1)} fusion(bf16[1024,4096]{1,0:T(8,128)(2,1)} %all-gather.4.cloned.1.call-done, bf16[4096,768]{1,0:T(8,128)(2,1)} %all-gather.6.cloned.1.call-done), kind=kOutput, calls=%fused_computation.14 | convolution fusion | flops 6442450944 | bytes 17825792 | tf_op jit(solution)/shard_map/dot_general | solution.py:26
  178.1 59.5 %all-gather.8.cloned.1.call-done = bf16[4096,768]{1,0:T(8,128)(2,1)} async-done(((bf16[1024,768]{1,0:T(8,128)(2,1)}), bf16[4096,768]{1,0:T(8,128)(2,1)}) %all-gather.8.cloned.1.call-update) | async-done | bytes 6291472 | tf_op jit(solution)/shard_map/all_gather | solution.py:23
  237.6 0.0 copy-done.5
  237.6 0.0 copy-done.6
  237.6 12.1 %multiply_convert_fusion = bf16[1024,768]{1,0:T(8,128)(2,1)} fusion(f32[1024,768]{1,0:T(8,128)S(1)} %fusion.8, bf16[1024,4096]{1,0:T(8,128)(2,1)} %all-gather.4.cloned.1.call-done, bf16[4096,768]{1,0:T(8,128)(2,1)} %all-gather.8.cloned.1.call-done, f32[768]{0:T(1024)S(1)} %copy-done.5, f32[768]{0:T(1024)S(1)} %copy-done.6), kind=kOutput, calls=%fused_computation | convolution fusion | flops 6448742400 | bytes 19404800 | tf_op jit(solution)/shard_map/dot_general | solution.py:27
  (2 shorter events, 0.0 us)
Async XLA Ops:
  7.2 3.5 %copy-start.1 = (bf16[128,4096]{1,0:T(8,128)(2,1)S(1)}, bf16[128,4096]{1,0:T(8,128)(2,1)}, u32[]{:S(2)}) copy-start(bf16[128,4096]{1,0:T(8,128)(2,1)} %param.9) | copy-start | bytes 3145732
  7.2 3.8 %copy-start.3 = (f32[4096]{0:T(1024)S(1)}, f32[4096]{0:T(1024)}, u32[]{:S(2)}) copy-start(f32[4096]{0:T(1024)} %param.10) | copy-start | bytes 49156
  7.2 3.8 %copy-start.2 = (bf16[128,4096]{1,0:T(8,128)(2,1)S(1)}, bf16[128,4096]{1,0:T(8,128)(2,1)}, u32[]{:S(2)}) copy-start(bf16[128,4096]{1,0:T(8,128)(2,1)} %param.8) | copy-start | bytes 3145732
  7.2 76.3 %all-gather.6.cloned.1.call-start = ((), (), s32[]{:S(2)}) async-start(), calls=%async_computation.1 | async-start | bytes 7864320 | tf_op jit(solution)/shard_map/all_gather | solution.py:22
  10.6 1.2 copy-start.4
  10.6 156.6 %all-gather.4.cloned.1.call-start = ((), (), s32[]{:S(2)}) async-start(), calls=%async_computation | async-start | bytes 9437184 | tf_op jit(solution)/shard_map/all_gather | solution.py:25
  11.7 4.7 %copy-start = (bf16[128,4096]{1,0:T(8,128)(2,1)}, bf16[128,4096]{1,0:T(8,128)(2,1)S(1)}, u32[]{:S(2)}) copy-start(bf16[128,4096]{1,0:T(8,128)(2,1)S(1)} %get-tuple-element.3) | copy-start | bytes 3145732
  13.1 224.4 %all-gather.8.cloned.1.call-start = ((), (), s32[]{:S(2)}) async-start(), calls=%async_computation.2 | async-start | bytes 7864320 | tf_op jit(solution)/shard_map/all_gather | solution.py:23
  16.4 221.2 %copy-start.5 = (f32[768]{0:T(1024)S(1)}, f32[768]{0:T(1024)}, u32[]{:S(2)}) copy-start(f32[768]{0:T(1024)} %param.15) | copy-start | bytes 9220
  16.4 221.1 %copy-start.6 = (f32[768]{0:T(1024)S(1)}, f32[768]{0:T(1024)}, u32[]{:S(2)}) copy-start(f32[768]{0:T(1024)} %param.14) | copy-start | bytes 9220
Sparse Core Ops, SparseCore 0:
  10.7 72.7 all-gather.5
  85.1 82.0 all-gather.3
  169.0 68.5 all-gather.7
where the time goes:
time: 256 us
  waiting for transfers between devices  210 us (82%)
  matrix products  23 us (9%)
  between operations  13.8 us (5%)
  other arithmetic  8.92 us (3%)
    all_gather x1, waiting for transfers between devices, on_device(): piece = lax.all_gather(normed, 'tp', axis=0, tiled=True)  83.7 us
    all_gather x1, waiting for transfers between devices, on_device(): lax.all_gather(gate_cast, 'fs', axis=0, tiled=True)  67.1 us
    all_gather x1, waiting for transfers between devices, on_device(): lax.all_gather(up_cast, 'fs', axis=0, tiled=True)  59.5 us
    dot_general x1, matrix products, on_device(): up = jnp.dot(piece, up_full, preferred_element_type=jnp.float32) * up_scale  12.1 us
    dot_general x1, matrix products, on_device(): jnp.dot(piece, gate_full, preferred_element_type=jnp.float32) * gate_scale  10.9 us
  transfers between devices with their start and end apart: 3, of which 3 were waited for; matrix products, arithmetic and copies ran while one was open for 6% of the time, Pallas kernels for 0%

commit v1 on v0

v1 whole, which is shorter than its diff:
```python
import math

import jax
import jax.numpy as jnp
from jax import lax
from jax.experimental import pallas as pl
from jax.experimental.pallas import tpu as pltpu
from jax.sharding import PartitionSpec as P


epsilon = 1e-06
CHUNK = 128
ANY = pl.BlockSpec(memory_space=pltpu.HBM)


def rms_scaled(values, gain):
    return values * lax.rsqrt(jnp.mean(values * values, axis=-1, keepdims=True) + epsilon) * gain


def cast(gate_weight, up_weight, j, c):
    k = gate_weight.shape[0]

    def body(g, u, top, bottom):
        for half, out in enumerate((top, bottom)):
            rows = slice(half * (k // 2), (half + 1) * (k // 2))
            out[:, :c] = g[rows].astype(out.dtype)
            out[:, c:] = u[rows].astype(out.dtype)

    spec = pl.BlockSpec((k, c), lambda i: (0, j))
    whole = pl.BlockSpec((k // 2, 2 * c), lambda i: (0, 0))
    shape = jax.ShapeDtypeStruct((k // 2, 2 * c), jnp.bfloat16)
    return pl.pallas_call(
        body, grid=(1,), in_specs=[spec, spec], out_specs=[whole, whole], out_shape=[shape, shape]
    )(gate_weight, up_weight)


def pack(gate_scale, up_scale):
    def body(g, u, out):
        out[0:1] = g[...]
        out[1:2] = u[...]

    return pl.pallas_call(
        body,
        out_shape=jax.ShapeDtypeStruct((2, gate_scale.shape[1]), jnp.float32),
        name="pack",
    )(gate_scale, up_scale)


def assemble(slots, mates, chips):
    rows, width = slots[0].shape
    n = 2 * chips - 1

    def body(*refs):
        out, sem = refs[2 * n], refs[2 * n + 1]
        t = lax.axis_index("tp")
        z, core = t // 2, t % 2

        def copies(fn):
            for side in range(2):
                for i in range(n):
                    source = z + i - (chips - 1)

                    @pl.when((source >= 0) & (source < chips))
                    def _():
                        lane = core if side == 0 else 1 - core
                        at = pl.multiple_of((2 * source + lane) * rows, rows)
                        fn(
                            pltpu.make_async_copy(
                                refs[side * n + i], out.at[pl.ds(at, rows)], sem.at[side, i]
                            )
                        )

        copies(lambda c: c.start())
        copies(lambda c: c.wait())

    return pl.pallas_call(
        body,
        in_specs=[ANY] * (2 * n),
        out_specs=ANY,
        out_shape=jax.ShapeDtypeStruct((2 * chips * rows, width), slots[0].dtype),
        scratch_shapes=[pltpu.SemaphoreType.DMA((2, n))],
        name="assemble",
    )(*slots, *mates)


def project(tokens, pieces, scales, hidden, index, fa, fb, width):
    m, k = tokens.shape
    half, two_c = pieces[0][3].shape
    c = two_c // 2
    tm = min(256, m)
    n = len(pieces)

    def body(a, scale, *rest):
        parts, rest = rest[:n], rest[n:]
        if hidden is not None:
            rest = rest[1:]
        out, w, sem = rest

        @pl.when(pl.program_id(0) == 0)
        def _():
            f = lax.axis_index("fs")
            y, x = f // fa, f % fa

            def copy(i):
                h, dx, dy, _ = pieces[i]
                owner = ((y + fb - dy) % fb) * fa + (x + fa - dx) % fa
                at = pl.multiple_of((2 * owner + h) * half, half)
                return pltpu.make_async_copy(parts[i], w.at[pl.ds(at, half)], sem.at[i])

            for i in range(n):
                copy(i).start()
            for i in range(n):
                copy(i).wait()

        both = jnp.dot(a[...], w[...], preferred_element_type=jnp.float32)
        gate = both[:, :c] * scale[0:1]
        up = both[:, c:] * scale[1:2]
        out[...] = (gate / (1.0 + jnp.exp(-gate)) * up).astype(out.dtype)

    in_specs = [
        pl.BlockSpec((tm, k), lambda i: (i, 0)),
        pl.BlockSpec((2, c), lambda i: (0, index)),
    ] + [ANY] * n
    args = [tokens, scales] + [p[3] for p in pieces]
    aliases = {}
    if hidden is not None:
        aliases = {len(args): 0}
        in_specs.append(ANY)
        args.append(hidden)
    return pl.pallas_call(
        body,
        grid=(m // tm,),
        in_specs=in_specs,
        out_specs=pl.BlockSpec((tm, c), lambda i: (i, index)),
        out_shape=jax.ShapeDtypeStruct((m, width), jnp.bfloat16),
        scratch_shapes=[pltpu.VMEM((k, two_c), jnp.bfloat16), pltpu.SemaphoreType.DMA((n,))],
        input_output_aliases=aliases,
        cost_estimate=pl.CostEstimate(
            flops=2 * m * k * two_c,
            bytes_accessed=2 * (m * k + k * two_c + m * c),
            transcendentals=m * c,
        ),
    )(*args)


def solution(mesh):
    fs, tp = mesh.shape["fs"], mesh.shape["tp"]
    fa = math.isqrt(fs)
    fb = fs // fa
    chips = tp // 2
    along_x = [(y * fa + x, y * fa + (x + 1) % fa) for y in range(fb) for x in range(fa)]
    along_y = [(y * fa + x, ((y + 1) % fb) * fa + x) for y in range(fb) for x in range(fa)]
    swap = [(t, t ^ 1) for t in range(tp)]

    def ring(values, pairs, count):
        found = [values]
        for _ in range(count - 1):
            values = [lax.ppermute(v, "fs", pairs) for v in values]
            found.append(values)
        return found

    def gather(top, bottom):
        pieces = []
        first = [step[0] for step in ring([top], along_x, fa)]
        here = ring(first[:1], along_y, fb)
        there = ring(first[1:], along_y, fb)
        for dy in range(fb):
            pieces += [(0, dx, dy, v) for dx, v in enumerate(here[dy] + there[dy])]
        first = [step[0] for step in ring([bottom], along_y, fb)]
        here = ring(first[:1], along_x, fa)
        there = ring(first[1:], along_x, fa)
        for dx in range(fa):
            pieces += [(1, dx, dy, v) for dy, v in enumerate(here[dx] + there[dx])]
        return pieces

    def line(value):
        below, above = [], []
        low = high = value
        for s in range(1, chips):
            up = [(2 * z + c, 2 * z + 2 + c) for z in range(s - 1, chips - 1) for c in range(2)]
            down = [(2 * z + c, 2 * z - 2 + c) for z in range(1, chips - s + 1) for c in range(2)]
            low = lax.ppermute(low, "tp", up)
            high = lax.ppermute(high, "tp", down)
            below.append(low)
            above.append(high)
        return below[::-1] + [value] + above

    def on_device(
        stream_in, mixer_out, mix_gain, pre_gain, gate_weight, up_weight, gate_scale, up_scale
    ):
        mixed = stream_in.astype(jnp.float32) + rms_scaled(mixer_out.astype(jnp.float32), mix_gain)
        stream = mixed.astype(jnp.bfloat16)
        normed = rms_scaled(stream.astype(jnp.float32), pre_gain).astype(jnp.bfloat16)
        slots = line(normed)
        mates = []
        for v in slots:
            mates.append(lax.ppermute(v, "tp", swap))
        width = gate_weight.shape[1]
        gathered = []
        for j in range(width // CHUNK):
            top, bottom = cast(gate_weight, up_weight, j, CHUNK)
            gathered.append(gather(top, bottom))
        scales = pack(gate_scale[None], up_scale[None])
        tokens = assemble(slots, mates, chips)
        hidden = None
        for j, pieces in enumerate(gathered):
            hidden = project(tokens, pieces, scales, hidden, j, fa, fb, width)
        return (hidden, stream)

    return jax.shard_map(
        on_device,
        mesh=mesh,
        in_specs=(
            P(("fs", "tp"), None),
            P(("fs", "tp"), None),
            P(),
            P(),
            P("fs", "tp"),
            P("fs", "tp"),
            P("tp"),
            P("tp"),
        ),
        out_specs=(P("fs", "tp"), P(("fs", "tp"), None)),
        check_vma=False,
    )
```

time: 256 us -> 431 us (1.68)
  Pallas kernels: 0 us -> 317 us
  waiting for transfers between devices: 210 us -> 46.1 us
  starting transfers between devices: 0.12 us -> 56.6 us
  matrix products: 23 us -> 0 us
  between operations: 13.8 us -> 1.11 us
  other arithmetic: 8.92 us -> 4.16 us
    pallas_call x0 -> x14, Pallas kernels: none -> 317 us  [the longest x1 255 us: assemble(): pl.pallas_call(body, in_specs=[ANY] * (2 * n), out_specs=ANY, out_shape=j...]
    all_gather x3 -> x0, waiting for transfers between devices: 210 us -> none  [the longest x1 83.7 us: on_device(): piece = lax.all_gather(normed, 'tp', axis=0, tiled=True)]
    ppermute x0 -> x49, starting transfers between devices: none -> 56.6 us  [the longest x36 41.6 us: ring(): values = [lax.ppermute(v, 'fs', pairs) for v in values]]
    ppermute x0 -> x49, waiting for transfers between devices: none -> 46.1 us  [the longest x36 44.1 us: ring(): values = [lax.ppermute(v, 'fs', pairs) for v in values]]
    dot_general x2 -> x0, matrix products: 23 us -> none  [the longest x1 12.1 us: on_device(): up = jnp.dot(piece, up_full, preferred_element_type=jnp.float32) * up_scale]
    convert_element_type x2 -> x0, other arithmetic: 6.54 us -> none  [the longest x1 3.32 us: on_device(): gate_cast = gate_weight.astype(jnp.bfloat16)]
  transfers between devices with their start and end apart: 3 -> 49, of which waited for: 3 -> 15; matrix products, arithmetic and copies ran while one was open for 6% -> 0% of each run, Pallas kernels for 0% -> 72%
where the time goes in v1:
time: 431 us; the launch traced here: 428 us
  Pallas kernels  317 us (74%)
  starting transfers between devices  56.6 us (13%)
  waiting for transfers between devices  46.1 us (11%)
    pallas_call x1, Pallas kernels, assemble(): pl.pallas_call(body, in_specs=[ANY] * (2 * n), out_specs=ANY, out_shape=j...  255 us
    pallas_call x6, Pallas kernels, project(): pl.pallas_call(body, grid=(m // tm,), in_specs=in_specs, out_specs=pl.Blo...  47.7 us
    ppermute x36, waiting for transfers between devices, ring(): values = [lax.ppermute(v, 'fs', pairs) for v in values]  44.1 us
    ppermute x36, starting transfers between devices, ring(): values = [lax.ppermute(v, 'fs', pairs) for v in values]  41.6 us
    pallas_call x6, Pallas kernels, cast(): pl.pallas_call(body, grid=(1,), in_specs=[spec, spec], out_specs=[whole,...  12.3 us
    ppermute x3, starting transfers between devices, line(): low = lax.ppermute(low, 'tp', up)  9.94 us
  transfers between devices with their start and end apart: 49, of which 15 were waited for; matrix products, arithmetic and copies ran while one was open for 0% of the time, Pallas kernels for 72%

profile of v1, /device:TPU:0, one launch (start us, length us, event | category | flops | bytes accessed | tf_op | source)
XLA Modules:
  0.0 428.2 jit_solution(18338843704785603103)
XLA Ops:
  0.6 1.5 fusion
  2.2 2.3 fusion.4
  6.2 6.6 %collective-permute-start = (bf16[128,4096]{1,0:T(8,128)(2,1)S(1)}, bf16[128,4096]{1,0:T(8,128)(2,1)}, u32[]{:S(2)}, u32[]{:S(2)}) collective-permute-start(bf16[128,4096]{1,0:T(8,128)(2,1)S(1)} %fusion.6.refs_3_), channel_id=1, source_target_pairs={{0,2},{1,3},{2,4},{3,5},{4,6},{5,7},{8,10},{9,11},{10,12},{11,13},... | collective-permute-start | bytes 3145736 | tf_op jit(solution)/shard_map/ppermute | solution.py:182
  12.7 2.0 shard_map.100
  14.8 1.9 collective-permute-start.43
  16.7 1.5 collective-permute-start.46
  18.7 4.0 collective-permute-done.43.rest_1_
  22.8 1.6 collective-permute-start.47
  24.4 2.1 shard_map.99
  26.9 2.8 collective-permute-done.44.rest_2_
  29.7 1.5 collective-permute-start.40
  32.1 1.4 collective-permute-start.38
  33.5 2.0 collective-permute-done.37.rest_1_
  35.5 1.4 collective-permute-start.41
  38.2 1.6 collective-permute-start.1
  39.8 2.0 shard_map.98
  42.6 1.4 collective-permute-start.34
  44.6 4.7 %collective-permute-done.31.rest_1_ = bf16[512,256]{1,0:T(8,128)(2,1)} collective-permute-done((bf16[512,256]{1,0:T(8,128)(2,1)}, bf16[512,256]{1,0:T(8,128)(2,1)}, u32[]{:S(2)}, u32[]{:S(2)}) %collective-permute-start.31) | collective-permute-done | bytes 262176 | tf_op jit(solution)/shard_map/ppermute | solution.py:158
  49.2 2.1 shard_map.97
  51.3 2.0 collective-permute-start.25
  54.6 1.4 collective-permute-start.28
  57.0 1.5 collective-permute-start.26
  58.5 2.8 collective-permute-done.25.rest_1_
  61.3 2.0 shard_map.96
  63.4 2.0 collective-permute-start.19
  65.4 1.3 collective-permute-done.26.rest_2_
  66.7 1.4 collective-permute-start.22
  68.2 2.8 collective-permute-done.19.rest_1_
  72.4 1.7 collective-permute-start.2
  74.1 1.5 collective-permute-start.20
  75.6 7.4 %collective-permute-done.20.rest_2_ = bf16[512,256]{1,0:T(8,128)(2,1)S(1)} collective-permute-done((bf16[512,256]{1,0:T(8,128)(2,1)}, bf16[512,256]{1,0:T(8,128)(2,1)S(1)}, u32[]{:S(2)}, u32[]{:S(2)}) %collective-permute-start.20) | collective-permute-done | bytes 262176 | tf_op jit(solution)/shard_map/ppermute | solution.py:158
  84.0 7.1 %collective-permute-done.23.rest_6_ = bf16[512,256]{1,0:T(8,128)(2,1)S(1)} collective-permute-done((bf16[512,256]{1,0:T(8,128)(2,1)}, bf16[512,256]{1,0:T(8,128)(2,1)S(1)}, u32[]{:S(2)}, u32[]{:S(2)}) %collective-permute-start.23) | collective-permute-done | bytes 262176 | tf_op jit(solution)/shard_map/ppermute | solution.py:158
  91.2 1.5 collective-permute-start.45
  92.7 5.9 %collective-permute-done.45.rest_3_ = bf16[512,256]{1,0:T(8,128)(2,1)S(1)} collective-permute-done((bf16[512,256]{1,0:T(8,128)(2,1)}, bf16[512,256]{1,0:T(8,128)(2,1)S(1)}, u32[]{:S(2)}, u32[]{:S(2)}) %collective-permute-start.45) | collective-permute-done | bytes 262176 | tf_op jit(solution)/shard_map/ppermute | solution.py:158
  99.2 2.0 collective-permute-done.5.refs_6_
  101.7 1.3 collective-permute-start.48
  103.1 2.0 shard_map.95
  106.0 1.6 collective-permute-start.39
  111.8 255.3 %assemble.1.a = bf16[1024,4096]{1,0:T(8,128)(2,1)} custom-call(bf16[128,4096]{1,0:T(8,128)(2,1)} %collective-permute-done.2.refs_0_, bf16[128,4096]{1,0:T(8,128)(2,1)} %collective-permute-done.1.refs_1_, bf16[128,4096]{1,0:T(8,128)(2,1)} %collective-permute-done.refs_2_, bf16[128,4096]{1,0:T(8,128)(2,1)} %copy-done, bf16[128,4096]{1,0:T(8,128)(2,1)} %copy-done.2, ...), custom_call_target="tpu_custom_call" | custom-call | tf_op jit(solution)/shard_map/assemble/pallas_call | solution.py:76
  368.0 8.0 %shard_map.101.rest_8_ = bf16[1024,768]{1,0:T(8,128)(2,1)} custom-call(bf16[1024,4096]{1,0:T(8,128)(2,1)} %assemble.1.a, f32[2,768]{1,0:T(2,128)} %pack.1.scale, bf16[512,256]{1,0:T(8,128)(2,1)} %get-tuple-element.24.rest_0_, bf16[512,256]{1,0:T(8,128)(2,1)} %copy-done.9, bf16[512,256]{1,0:T(8,128)(2,1)} %copy-done.11, bf16[512,256]{1,0:T(8,128)(2,1)} %copy-done.21, ...), custom_call_target="tpu_custom_call" | custom-call | flops 2147483648 | bytes 10747904 | tf_op jit(solution)/shard_map/pallas_call | solution.py:130
  376.0 1.5 collective-permute-start.16
  379.3 1.5 collective-permute-start.21
  380.9 8.0 %shard_map.102.rest_8_ = bf16[1024,768]{1,0:T(8,128)(2,1)} custom-call(bf16[1024,4096]{1,0:T(8,128)(2,1)} %assemble.1.a, f32[2,768]{1,0:T(2,128)} %pack.1.scale, bf16[512,256]{1,0:T(8,128)(2,1)} %get-tuple-element.22.rest_0_, bf16[512,256]{1,0:T(8,128)(2,1)} %copy-done.8, ...), custom_call_target="tpu_custom_call", output_to_operand_aliasing={{}: (10, {})} | custom-call | flops 2147483648 | bytes 10747904 | tf_op jit(solution)/shard_map/pallas_call | solution.py:130
  389.7 7.9 %shard_map.103.rest_8_ = bf16[1024,768]{1,0:T(8,128)(2,1)} custom-call(bf16[1024,4096]{1,0:T(8,128)(2,1)} %assemble.1.a, f32[2,768]{1,0:T(2,128)} %pack.1.scale, bf16[512,256]{1,0:T(8,128)(2,1)} %get-tuple-element.20.rest_0_, bf16[512,256]{1,0:T(8,128)(2,1)} %collective-permute-done.31.rest_1_, ...), custom_call_target="tpu_custom_call", output_to_operand_aliasing={{}: (10, {})} | custom-call | flops 2147483648 | bytes 10747904 | tf_op jit(solution)/shard_map/pallas_call | solution.py:130
  399.6 1.6 collective-permute-start.15
  401.9 8.0 %shard_map.104.rest_8_ = bf16[1024,768]{1,0:T(8,128)(2,1)} custom-call(bf16[1024,4096]{1,0:T(8,128)(2,1)} %assemble.1.a, f32[2,768]{1,0:T(2,128)} %pack.1.scale, bf16[512,256]{1,0:T(8,128)(2,1)} %get-tuple-element.18.rest_0_, bf16[512,256]{1,0:T(8,128)(2,1)} %collective-permute-done.25.rest_1_, ...), custom_call_target="tpu_custom_call", output_to_operand_aliasing={{}: (10, {})} | custom-call | flops 2147483648 | bytes 10747904 | tf_op jit(solution)/shard_map/pallas_call | solution.py:130
  410.7 8.0 %shard_map.105.rest_8_ = bf16[1024,768]{1,0:T(8,128)(2,1)} custom-call(bf16[1024,4096]{1,0:T(8,128)(2,1)} %assemble.1.a, f32[2,768]{1,0:T(2,128)} %pack.1.scale, bf16[512,256]{1,0:T(8,128)(2,1)} %get-tuple-element.16.rest_0_, bf16[512,256]{1,0:T(8,128)(2,1)} %collective-permute-done.19.rest_1_, ...), custom_call_target="tpu_custom_call", output_to_operand_aliasing={{}: (10, {})} | custom-call | flops 2147483648 | bytes 10747904 | tf_op jit(solution)/shard_map/pallas_call | solution.py:130
  420.2 7.9 %shard_map.106 = bf16[1024,768]{1,0:T(8,128)(2,1)} custom-call(bf16[1024,4096]{1,0:T(8,128)(2,1)} %assemble.1.a, f32[2,768]{1,0:T(2,128)} %pack.1.scale, bf16[512,256]{1,0:T(8,128)(2,1)} %get-tuple-element.14.rest_0_, bf16[512,256]{1,0:T(8,128)(2,1)} %copy-done.19, bf16[512,256]{1,0:T(8,128)(2,1)} %copy-done.29, ...), custom_call_target="tpu_custom_call", output_to_operand_aliasing={{}: (10, {})} | custom-call | flops 2147483648 | bytes 10747904 | tf_op jit(solution)/shard_map/pallas_call | solution.py:130
  (145 shorter events, 25.5 us)
Async XLA Ops:
  4.9 32.0 %collective-permute-start.3 = (bf16[128,4096]{1,0:T(8,128)(2,1)S(1)}, bf16[128,4096]{1,0:T(8,128)(2,1)S(1)}, u32[]{:S(2)}, u32[]{:S(2)}) collective-permute-start(bf16[128,4096]{1,0:T(8,128)(2,1)S(1)} %fusion.6.refs_3_), channel_id=1, source_target_pairs={{2,0},{3,1},{4,2},{5,3},{6,4},{7,5},{10,8},{11,9},{12,10},{13,11},... | collective-permute-start | bytes 3145736 | tf_op jit(solution)/shard_map/ppermute | solution.py:183
  6.2 32.0 %collective-permute-start = (bf16[128,4096]{1,0:T(8,128)(2,1)S(1)}, bf16[128,4096]{1,0:T(8,128)(2,1)}, u32[]{:S(2)}, u32[]{:S(2)}) collective-permute-start(bf16[128,4096]{1,0:T(8,128)(2,1)S(1)} %fusion.6.refs_3_), channel_id=1, source_target_pairs={{0,2},{1,3},{2,4},{3,5},{4,6},{5,7},{8,10},{9,11},{10,12},{11,13},... | collective-permute-start | bytes 3145736 | tf_op jit(solution)/shard_map/ppermute | solution.py:182
  14.8 8.0 %collective-permute-start.43 = (bf16[512,256]{1,0:T(8,128)(2,1)}, bf16[512,256]{1,0:T(8,128)(2,1)S(1)}, u32[]{:S(2)}, u32[]{:S(2)}) collective-permute-start(bf16[512,256]{1,0:T(8,128)(2,1)} %get-tuple-element.24.rest_0_), channel_id=1, source_target_pairs={{0,8},{8,0},{16,24},{24,16},{1,9},{9,1},{17,25},{25,17},{2,10},{10... | collective-permute-start | bytes 786440 | tf_op jit(solution)/shard_map/ppermute | solution.py:158
  16.7 9.8 %collective-permute-start.46 = (bf16[512,256]{1,0:T(8,128)(2,1)}, bf16[512,256]{1,0:T(8,128)(2,1)S(1)}, u32[]{:S(2)}, u32[]{:S(2)}) collective-permute-start(bf16[512,256]{1,0:T(8,128)(2,1)} %get-tuple-element.25.rest_4_), channel_id=1, source_target_pairs={{0,16},{8,24},{16,0},{24,8},{1,17},{9,25},{17,1},{25,9},{2,18},{10... | collective-permute-start | bytes 786440 | tf_op jit(solution)/shard_map/ppermute | solution.py:158
  18.2 11.5 %collective-permute-start.44 = (bf16[512,256]{1,0:T(8,128)(2,1)}, bf16[512,256]{1,0:T(8,128)(2,1)S(1)}, u32[]{:S(2)}, u32[]{:S(2)}) collective-permute-start(bf16[512,256]{1,0:T(8,128)(2,1)} %get-tuple-element.24.rest_0_), channel_id=1, source_target_pairs={{0,16},{8,24},{16,0},{24,8},{1,17},{9,25},{17,1},{25,9},{2,18},{10... | collective-permute-start | bytes 786440 | tf_op jit(solution)/shard_map/ppermute | solution.py:158
  22.8 9.4 %collective-permute-start.47 = (bf16[512,256]{1,0:T(8,128)(2,1)}, bf16[512,256]{1,0:T(8,128)(2,1)S(1)}, u32[]{:S(2)}, u32[]{:S(2)}) collective-permute-start(bf16[512,256]{1,0:T(8,128)(2,1)} %get-tuple-element.25.rest_4_), channel_id=1, source_target_pairs={{0,8},{8,0},{16,24},{24,16},{1,9},{9,1},{17,25},{25,17},{2,10},{10... | collective-permute-start | bytes 786440 | tf_op jit(solution)/shard_map/ppermute | solution.py:158
  26.5 9.0 %collective-permute-start.37 = (bf16[512,256]{1,0:T(8,128)(2,1)}, bf16[512,256]{1,0:T(8,128)(2,1)S(1)}, u32[]{:S(2)}, u32[]{:S(2)}) collective-permute-start(bf16[512,256]{1,0:T(8,128)(2,1)} %get-tuple-element.22.rest_0_), channel_id=1, source_target_pairs={{0,8},{8,0},{16,24},{24,16},{1,9},{9,1},{17,25},{25,17},{2,10},{10... | collective-permute-start | bytes 786440 | tf_op jit(solution)/shard_map/ppermute | solution.py:158
  29.7 12.1 %collective-permute-start.40 = (bf16[512,256]{1,0:T(8,128)(2,1)}, bf16[512,256]{1,0:T(8,128)(2,1)}, u32[]{:S(2)}, u32[]{:S(2)}) collective-permute-start(bf16[512,256]{1,0:T(8,128)(2,1)} %get-tuple-element.23.rest_4_), channel_id=1, source_target_pairs={{0,16},{8,24},{16,0},{24,8},{1,17},{9,25},{17,1},{25,9},{2,18},{10... | collective-permute-start | bytes 786440 | tf_op jit(solution)/shard_map/ppermute | solution.py:158
  32.1 10.4 %collective-permute-start.38 = (bf16[512,256]{1,0:T(8,128)(2,1)}, bf16[512,256]{1,0:T(8,128)(2,1)}, u32[]{:S(2)}, u32[]{:S(2)}) collective-permute-start(bf16[512,256]{1,0:T(8,128)(2,1)} %get-tuple-element.22.rest_0_), channel_id=1, source_target_pairs={{0,16},{8,24},{16,0},{24,8},{1,17},{9,25},{17,1},{25,9},{2,18},{10... | collective-permute-start | bytes 786440 | tf_op jit(solution)/shard_map/ppermute | solution.py:158
  35.5 8.5 %collective-permute-start.41 = (bf16[512,256]{1,0:T(8,128)(2,1)}, bf16[512,256]{1,0:T(8,128)(2,1)}, u32[]{:S(2)}, u32[]{:S(2)}) collective-permute-start(bf16[512,256]{1,0:T(8,128)(2,1)} %get-tuple-element.23.rest_4_), channel_id=1, source_target_pairs={{0,8},{8,0},{16,24},{24,16},{1,9},{9,1},{17,25},{25,17},{2,10},{10... | collective-permute-start | bytes 786440 | tf_op jit(solution)/shard_map/ppermute | solution.py:158
  36.9 34.2 %collective-permute-start.4 = (bf16[128,4096]{1,0:T(8,128)(2,1)S(1)}, bf16[128,4096]{1,0:T(8,128)(2,1)S(1)}, u32[]{:S(2)}, u32[]{:S(2)}) collective-permute-start(bf16[128,4096]{1,0:T(8,128)(2,1)S(1)} %collective-permute-done.3.refs_4_), channel_id=1, source_target_pairs={{2,0},{3,1},{4,2},{5,3},{10,8},{11,9},{12,10},{13,11},{18,16},{19,... | collective-permute-start | bytes 3145736 | tf_op jit(solution)/shard_map/ppermute | solution.py:183
  38.2 34.2 %collective-permute-start.1 = (bf16[128,4096]{1,0:T(8,128)(2,1)}, bf16[128,4096]{1,0:T(8,128)(2,1)}, u32[]{:S(2)}, u32[]{:S(2)}) collective-permute-start(bf16[128,4096]{1,0:T(8,128)(2,1)} %collective-permute-done.refs_2_), channel_id=1, source_target_pairs={{2,4},{3,5},{4,6},{5,7},{10,12},{11,13},{12,14},{13,15},{18,20},{1... | collective-permute-start | bytes 3145736 | tf_op jit(solution)/shard_map/ppermute | solution.py:182
  41.9 7.4 %collective-permute-start.31 = (bf16[512,256]{1,0:T(8,128)(2,1)}, bf16[512,256]{1,0:T(8,128)(2,1)}, u32[]{:S(2)}, u32[]{:S(2)}) collective-permute-start(bf16[512,256]{1,0:T(8,128)(2,1)} %get-tuple-element.20.rest_0_), channel_id=1, source_target_pairs={{0,8},{8,0},{16,24},{24,16},{1,9},{9,1},{17,25},{25,17},{2,10},{10... | collective-permute-start | bytes 786440 | tf_op jit(solution)/shard_map/ppermute | solution.py:158
  42.6 8.8 %collective-permute-start.34 = (bf16[512,256]{1,0:T(8,128)(2,1)}, bf16[512,256]{1,0:T(8,128)(2,1)}, u32[]{:S(2)}, u32[]{:S(2)}) collective-permute-start(bf16[512,256]{1,0:T(8,128)(2,1)} %get-tuple-element.21.rest_4_), channel_id=1, source_target_pairs={{0,16},{8,24},{16,0},{24,8},{1,17},{9,25},{17,1},{25,9},{2,18},{10... | collective-permute-start | bytes 786440 | tf_op jit(solution)/shard_map/ppermute | solution.py:158
  44.0 10.7 %collective-permute-start.32 = (bf16[512,256]{1,0:T(8,128)(2,1)}, bf16[512,256]{1,0:T(8,128)(2,1)}, u32[]{:S(2)}, u32[]{:S(2)}) collective-permute-start(bf16[512,256]{1,0:T(8,128)(2,1)} %get-tuple-element.20.rest_0_), channel_id=1, source_target_pairs={{0,16},{8,24},{16,0},{24,8},{1,17},{9,25},{17,1},{25,9},{2,18},{10... | collective-permute-start | bytes 786440 | tf_op jit(solution)/shard_map/ppermute | solution.py:158
  49.2 7.8 %collective-permute-start.35 = (bf16[512,256]{1,0:T(8,128)(2,1)}, bf16[512,256]{1,0:T(8,128)(2,1)}, u32[]{:S(2)}, u32[]{:S(2)}) collective-permute-start(bf16[512,256]{1,0:T(8,128)(2,1)} %get-tuple-element.21.rest_4_), channel_id=1, source_target_pairs={{0,8},{8,0},{16,24},{24,16},{1,9},{9,1},{17,25},{25,17},{2,10},{10... | collective-permute-start | bytes 786440 | tf_op jit(solution)/shard_map/ppermute | solution.py:158
  51.3 10.0 %collective-permute-start.25 = (bf16[512,256]{1,0:T(8,128)(2,1)}, bf16[512,256]{1,0:T(8,128)(2,1)}, u32[]{:S(2)}, u32[]{:S(2)}) collective-permute-start(bf16[512,256]{1,0:T(8,128)(2,1)} %get-tuple-element.18.rest_0_), channel_id=1, source_target_pairs={{0,8},{8,0},{16,24},{24,16},{1,9},{9,1},{17,25},{25,17},{2,10},{10... | collective-permute-start | bytes 786440 | tf_op jit(solution)/shard_map/ppermute | solution.py:158
  54.6 8.7 %collective-permute-start.28 = (bf16[512,256]{1,0:T(8,128)(2,1)}, bf16[512,256]{1,0:T(8,128)(2,1)}, u32[]{:S(2)}, u32[]{:S(2)}) collective-permute-start(bf16[512,256]{1,0:T(8,128)(2,1)} %get-tuple-element.19.rest_4_), channel_id=1, source_target_pairs={{0,16},{8,24},{16,0},{24,8},{1,17},{9,25},{17,1},{25,9},{2,18},{10... | collective-permute-start | bytes 786440 | tf_op jit(solution)/shard_map/ppermute | solution.py:158
  57.0 9.7 %collective-permute-start.26 = (bf16[512,256]{1,0:T(8,128)(2,1)}, bf16[512,256]{1,0:T(8,128)(2,1)}, u32[]{:S(2)}, u32[]{:S(2)}) collective-permute-start(bf16[512,256]{1,0:T(8,128)(2,1)} %get-tuple-element.18.rest_0_), channel_id=1, source_target_pairs={{0,16},{8,24},{16,0},{24,8},{1,17},{9,25},{17,1},{25,9},{2,18},{10... | collective-permute-start | bytes 786440 | tf_op jit(solution)/shard_map/ppermute | solution.py:158
  61.3 6.9 %collective-permute-start.29 = (bf16[512,256]{1,0:T(8,128)(2,1)}, bf16[512,256]{1,0:T(8,128)(2,1)}, u32[]{:S(2)}, u32[]{:S(2)}) collective-permute-start(bf16[512,256]{1,0:T(8,128)(2,1)} %get-tuple-element.19.rest_4_), channel_id=1, source_target_pairs={{0,8},{8,0},{16,24},{24,16},{1,9},{9,1},{17,25},{25,17},{2,10},{10... | collective-permute-start | bytes 786440 | tf_op jit(solution)/shard_map/ppermute | solution.py:158
  63.4 7.7 %collective-permute-start.19 = (bf16[512,256]{1,0:T(8,128)(2,1)}, bf16[512,256]{1,0:T(8,128)(2,1)}, u32[]{:S(2)}, u32[]{:S(2)}) collective-permute-start(bf16[512,256]{1,0:T(8,128)(2,1)} %get-tuple-element.16.rest_0_), channel_id=1, source_target_pairs={{0,8},{8,0},{16,24},{24,16},{1,9},{9,1},{17,25},{25,17},{2,10},{10... | collective-permute-start | bytes 786440 | tf_op jit(solution)/shard_map/ppermute | solution.py:158
  66.7 7.4 %collective-permute-start.22 = (bf16[512,256]{1,0:T(8,128)(2,1)}, bf16[512,256]{1,0:T(8,128)(2,1)S(1)}, u32[]{:S(2)}, u32[]{:S(2)}) collective-permute-start(bf16[512,256]{1,0:T(8,128)(2,1)} %get-tuple-element.17.rest_4_), channel_id=1, source_target_pairs={{0,16},{8,24},{16,0},{24,8},{1,17},{9,25},{17,1},{25,9},{2,18},{10... | collective-permute-start | bytes 786440 | tf_op jit(solution)/shard_map/ppermute | solution.py:158
  68.2 30.3 %collective-permute-start.9 = (bf16[128,4096]{1,0:T(8,128)(2,1)S(1)}, bf16[128,4096]{1,0:T(8,128)(2,1)S(1)}, u32[]{:S(2)}, u32[]{:S(2)}) collective-permute-start(bf16[128,4096]{1,0:T(8,128)(2,1)S(1)} %fusion.6.refs_3_), channel_id=1, source_target_pairs={{0,1},{1,0},{2,3},{3,2},{4,5},{5,4},{6,7},{7,6},{8,9},{9,8},{10,11... | collective-permute-start | bytes 3145736 | tf_op jit(solution)/shard_map/ppermute | solution.py:197
  71.1 28.0 %collective-permute-start.10 = (bf16[128,4096]{1,0:T(8,128)(2,1)S(1)}, bf16[128,4096]{1,0:T(8,128)(2,1)S(1)}, u32[]{:S(2)}, u32[]{:S(2)}) collective-permute-start(bf16[128,4096]{1,0:T(8,128)(2,1)S(1)} %collective-permute-done.3.refs_4_), channel_id=1, source_target_pairs={{0,1},{1,0},{2,3},{3,2},{4,5},{5,4},{6,7},{7,6},{8,9},{9,8},{10,11... | collective-permute-start | bytes 3145736 | tf_op jit(solution)/shard_map/ppermute | solution.py:197
  71.1 30.1 %collective-permute-start.5 = (bf16[128,4096]{1,0:T(8,128)(2,1)S(1)}, bf16[128,4096]{1,0:T(8,128)(2,1)}, u32[]{:S(2)}, u32[]{:S(2)}) collective-permute-start(bf16[128,4096]{1,0:T(8,128)(2,1)S(1)} %collective-permute-done.4.refs_5_), channel_id=1, source_target_pairs={{2,0},{3,1},{10,8},{11,9},{18,16},{19,17},{26,24},{27,25}} | collective-permute-start | bytes 3145736 | tf_op jit(solution)/shard_map/ppermute | solution.py:183
  72.4 28.8 %collective-permute-start.2 = (bf16[128,4096]{1,0:T(8,128)(2,1)}, bf16[128,4096]{1,0:T(8,128)(2,1)}, u32[]{:S(2)}, u32[]{:S(2)}) collective-permute-start(bf16[128,4096]{1,0:T(8,128)(2,1)} %collective-permute-done.1.refs_1_), channel_id=1, source_target_pairs={{4,6},{5,7},{12,14},{13,15},{20,22},{21,23},{28,30},{29,31}} | collective-permute-start | bytes 3145736 | tf_op jit(solution)/shard_map/ppermute | solution.py:182
  74.1 8.9 %collective-permute-start.20 = (bf16[512,256]{1,0:T(8,128)(2,1)}, bf16[512,256]{1,0:T(8,128)(2,1)S(1)}, u32[]{:S(2)}, u32[]{:S(2)}) collective-permute-start(bf16[512,256]{1,0:T(8,128)(2,1)} %get-tuple-element.16.rest_0_), channel_id=1, source_target_pairs={{0,16},{8,24},{16,0},{24,8},{1,17},{9,25},{17,1},{25,9},{2,18},{10... | collective-permute-start | bytes 786440 | tf_op jit(solution)/shard_map/ppermute | solution.py:158
  83.0 8.2 %collective-permute-start.23 = (bf16[512,256]{1,0:T(8,128)(2,1)}, bf16[512,256]{1,0:T(8,128)(2,1)S(1)}, u32[]{:S(2)}, u32[]{:S(2)}) collective-permute-start(bf16[512,256]{1,0:T(8,128)(2,1)} %get-tuple-element.17.rest_4_), channel_id=1, source_target_pairs={{0,8},{8,0},{16,24},{24,16},{1,9},{9,1},{17,25},{25,17},{2,10},{10... | collective-permute-start | bytes 786440 | tf_op jit(solution)/shard_map/ppermute | solution.py:158
  91.2 7.4 %collective-permute-start.45 = (bf16[512,256]{1,0:T(8,128)(2,1)}, bf16[512,256]{1,0:T(8,128)(2,1)S(1)}, u32[]{:S(2)}, u32[]{:S(2)}) collective-permute-start(bf16[512,256]{1,0:T(8,128)(2,1)} %copy-done.9), channel_id=1, source_target_pairs={{0,16},{8,24},{16,0},{24,8},{1,17},{9,25},{17,1},{25,9},{2,18},{10... | collective-permute-start | bytes 786440 | tf_op jit(solution)/shard_map/ppermute | solution.py:158
  98.6 6.5 %collective-permute-start.11 = (bf16[128,4096]{1,0:T(8,128)(2,1)S(1)}, bf16[128,4096]{1,0:T(8,128)(2,1)S(1)}, u32[]{:S(2)}, u32[]{:S(2)}) collective-permute-start(bf16[128,4096]{1,0:T(8,128)(2,1)S(1)} %collective-permute-done.4.refs_5_), channel_id=1, source_target_pairs={{0,1},{1,0},{2,3},{3,2},{4,5},{5,4},{6,7},{7,6},{8,9},{9,8},{10,11... | collective-permute-start | bytes 3145736 | tf_op jit(solution)/shard_map/ppermute | solution.py:197
  99.1 6.9 %collective-permute-start.7 = (bf16[128,4096]{1,0:T(8,128)(2,1)}, bf16[128,4096]{1,0:T(8,128)(2,1)S(1)}, u32[]{:S(2)}, u32[]{:S(2)}) collective-permute-start(bf16[128,4096]{1,0:T(8,128)(2,1)} %collective-permute-done.1.refs_1_), channel_id=1, source_target_pairs={{0,1},{1,0},{2,3},{3,2},{4,5},{5,4},{6,7},{7,6},{8,9},{9,8},{10,11... | collective-permute-start | bytes 3145736 | tf_op jit(solution)/shard_map/ppermute | solution.py:197
  101.1 6.4 %collective-permute-start.12 = (bf16[128,4096]{1,0:T(8,128)(2,1)}, bf16[128,4096]{1,0:T(8,128)(2,1)}, u32[]{:S(2)}, u32[]{:S(2)}) collective-permute-start(bf16[128,4096]{1,0:T(8,128)(2,1)} %collective-permute-done.5.refs_6_), channel_id=1, source_target_pairs={{0,1},{1,0},{2,3},{3,2},{4,5},{5,4},{6,7},{7,6},{8,9},{9,8},{10,11... | collective-permute-start | bytes 3145736 | tf_op jit(solution)/shard_map/ppermute | solution.py:197
  101.2 7.6 %collective-permute-start.6 = (bf16[128,4096]{1,0:T(8,128)(2,1)}, bf16[128,4096]{1,0:T(8,128)(2,1)}, u32[]{:S(2)}, u32[]{:S(2)}) collective-permute-start(bf16[128,4096]{1,0:T(8,128)(2,1)} %collective-permute-done.2.refs_0_), channel_id=1, source_target_pairs={{0,1},{1,0},{2,3},{3,2},{4,5},{5,4},{6,7},{7,6},{8,9},{9,8},{10,11... | collective-permute-start | bytes 3145736 | tf_op jit(solution)/shard_map/ppermute | solution.py:197
  101.7 265.4 %collective-permute-start.48 = (bf16[512,256]{1,0:T(8,128)(2,1)}, bf16[512,256]{1,0:T(8,128)(2,1)}, u32[]{:S(2)}, u32[]{:S(2)}) collective-permute-start(bf16[512,256]{1,0:T(8,128)(2,1)} %copy-done.10), channel_id=1, source_target_pairs={{0,8},{8,0},{16,24},{24,16},{1,9},{9,1},{17,25},{25,17},{2,10},{10... | collective-permute-start | bytes 786440 | tf_op jit(solution)/shard_map/ppermute | solution.py:158
  105.1 270.9 %collective-permute-start.13 = (bf16[512,256]{1,0:T(8,128)(2,1)}, bf16[512,256]{1,0:T(8,128)(2,1)S(1)}, u32[]{:S(2)}, u32[]{:S(2)}) collective-permute-start(bf16[512,256]{1,0:T(8,128)(2,1)} %get-tuple-element.14.rest_0_), channel_id=1, source_target_pairs={{0,8},{8,0},{16,24},{24,16},{1,9},{9,1},{17,25},{25,17},{2,10},{10... | collective-permute-start | bytes 786440 | tf_op jit(solution)/shard_map/ppermute | solution.py:158
  106.0 271.6 %collective-permute-start.39 = (bf16[512,256]{1,0:T(8,128)(2,1)S(1)}, bf16[512,256]{1,0:T(8,128)(2,1)S(1)}, u32[]{:S(2)}, u32[]{:S(2)}) collective-permute-start(bf16[512,256]{1,0:T(8,128)(2,1)S(1)} %collective-permute-done.37.rest_1_), channel_id=1, source_target_pairs={{0,16},{8,24},{16,0},{24,8},{1,17},{9,25},{17,1},{25,9},{2,18},{10... | collective-permute-start | bytes 786440 | tf_op jit(solution)/shard_map/ppermute | solution.py:158
  107.5 270.6 %collective-permute-start.42 = (bf16[512,256]{1,0:T(8,128)(2,1)}, bf16[512,256]{1,0:T(8,128)(2,1)S(1)}, u32[]{:S(2)}, u32[]{:S(2)}) collective-permute-start(bf16[512,256]{1,0:T(8,128)(2,1)} %collective-permute-done.40.rest_5_), channel_id=1, source_target_pairs={{0,8},{8,0},{16,24},{24,16},{1,9},{9,1},{17,25},{25,17},{2,10},{10... | collective-permute-start | bytes 786440 | tf_op jit(solution)/shard_map/ppermute | solution.py:158
  108.8 270.5 %collective-permute-start.33 = (bf16[512,256]{1,0:T(8,128)(2,1)}, bf16[512,256]{1,0:T(8,128)(2,1)S(1)}, u32[]{:S(2)}, u32[]{:S(2)}) collective-permute-start(bf16[512,256]{1,0:T(8,128)(2,1)} %collective-permute-done.31.rest_1_), channel_id=1, source_target_pairs={{0,16},{8,24},{16,0},{24,8},{1,17},{9,25},{17,1},{25,9},{2,18},{10... | collective-permute-start | bytes 786440 | tf_op jit(solution)/shard_map/ppermute | solution.py:158
  367.1 21.7 %collective-permute-start.36 = (bf16[512,256]{1,0:T(8,128)(2,1)}, bf16[512,256]{1,0:T(8,128)(2,1)S(1)}, u32[]{:S(2)}, u32[]{:S(2)}) collective-permute-start(bf16[512,256]{1,0:T(8,128)(2,1)} %collective-permute-done.34.rest_5_), channel_id=1, source_target_pairs={{0,8},{8,0},{16,24},{24,16},{1,9},{9,1},{17,25},{25,17},{2,10},{10... | collective-permute-start | bytes 786440 | tf_op jit(solution)/shard_map/ppermute | solution.py:158
  376.0 21.7 %collective-permute-start.16 = (bf16[512,256]{1,0:T(8,128)(2,1)S(1)}, bf16[512,256]{1,0:T(8,128)(2,1)S(1)}, u32[]{:S(2)}, u32[]{:S(2)}) collective-permute-start(bf16[512,256]{1,0:T(8,128)(2,1)S(1)} %copy-done.18), channel_id=1, source_target_pairs={{0,16},{8,24},{16,0},{24,8},{1,17},{9,25},{17,1},{25,9},{2,18},{10... | collective-permute-start | bytes 786440 | tf_op jit(solution)/shard_map/ppermute | solution.py:158
  377.6 20.8 %collective-permute-start.27 = (bf16[512,256]{1,0:T(8,128)(2,1)}, bf16[512,256]{1,0:T(8,128)(2,1)S(1)}, u32[]{:S(2)}, u32[]{:S(2)}) collective-permute-start(bf16[512,256]{1,0:T(8,128)(2,1)} %collective-permute-done.25.rest_1_), channel_id=1, source_target_pairs={{0,16},{8,24},{16,0},{24,8},{1,17},{9,25},{17,1},{25,9},{2,18},{10... | collective-permute-start | bytes 786440 | tf_op jit(solution)/shard_map/ppermute | solution.py:158
  378.1 21.4 %collective-permute-start.30 = (bf16[512,256]{1,0:T(8,128)(2,1)}, bf16[512,256]{1,0:T(8,128)(2,1)S(1)}, u32[]{:S(2)}, u32[]{:S(2)}) collective-permute-start(bf16[512,256]{1,0:T(8,128)(2,1)} %collective-permute-done.28.rest_5_), channel_id=1, source_target_pairs={{0,8},{8,0},{16,24},{24,16},{1,9},{9,1},{17,25},{25,17},{2,10},{10... | collective-permute-start | bytes 786440 | tf_op jit(solution)/shard_map/ppermute | solution.py:158
  379.3 21.8 %collective-permute-start.21 = (bf16[512,256]{1,0:T(8,128)(2,1)}, bf16[512,256]{1,0:T(8,128)(2,1)S(1)}, u32[]{:S(2)}, u32[]{:S(2)}) collective-permute-start(bf16[512,256]{1,0:T(8,128)(2,1)} %collective-permute-done.19.rest_1_), channel_id=1, source_target_pairs={{0,16},{8,24},{16,0},{24,8},{1,17},{9,25},{17,1},{25,9},{2,18},{10... | collective-permute-start | bytes 786440 | tf_op jit(solution)/shard_map/ppermute | solution.py:158
  388.9 21.0 %collective-permute-start.24 = (bf16[512,256]{1,0:T(8,128)(2,1)S(1)}, bf16[512,256]{1,0:T(8,128)(2,1)S(1)}, u32[]{:S(2)}, u32[]{:S(2)}) collective-permute-start(bf16[512,256]{1,0:T(8,128)(2,1)S(1)} %copy-done.14), channel_id=1, source_target_pairs={{0,8},{8,0},{16,24},{24,16},{1,9},{9,1},{17,25},{25,17},{2,10},{10... | collective-permute-start | bytes 786440 | tf_op jit(solution)/shard_map/ppermute | solution.py:158
  397.7 20.9 %collective-permute-start.14 = (bf16[512,256]{1,0:T(8,128)(2,1)S(1)}, bf16[512,256]{1,0:T(8,128)(2,1)S(1)}, u32[]{:S(2)}, u32[]{:S(2)}) collective-permute-start(bf16[512,256]{1,0:T(8,128)(2,1)S(1)} %copy-done.17), channel_id=1, source_target_pairs={{0,16},{8,24},{16,0},{24,8},{1,17},{9,25},{17,1},{25,9},{2,18},{10... | collective-permute-start | bytes 786440 | tf_op jit(solution)/shard_map/ppermute | solution.py:158
  398.3 20.3 %collective-permute-start.17 = (bf16[512,256]{1,0:T(8,128)(2,1)S(1)}, bf16[512,256]{1,0:T(8,128)(2,1)S(1)}, u32[]{:S(2)}, u32[]{:S(2)}) collective-permute-start(bf16[512,256]{1,0:T(8,128)(2,1)S(1)} %copy-done.18), channel_id=1, source_target_pairs={{0,8},{8,0},{16,24},{24,16},{1,9},{9,1},{17,25},{25,17},{2,10},{10... | collective-permute-start | bytes 786440 | tf_op jit(solution)/shard_map/ppermute | solution.py:158
  399.6 19.1 %collective-permute-start.15 = (bf16[512,256]{1,0:T(8,128)(2,1)S(1)}, bf16[512,256]{1,0:T(8,128)(2,1)S(1)}, u32[]{:S(2)}, u32[]{:S(2)}) collective-permute-start(bf16[512,256]{1,0:T(8,128)(2,1)S(1)} %collective-permute-done.13.rest_1_), channel_id=1, source_target_pairs={{0,16},{8,24},{16,0},{24,8},{1,17},{9,25},{17,1},{25,9},{2,18},{10... | collective-permute-start | bytes 786440 | tf_op jit(solution)/shard_map/ppermute | solution.py:158
  401.1 17.5 %collective-permute-start.18 = (bf16[512,256]{1,0:T(8,128)(2,1)S(1)}, bf16[512,256]{1,0:T(8,128)(2,1)S(1)}, u32[]{:S(2)}, u32[]{:S(2)}) collective-permute-start(bf16[512,256]{1,0:T(8,128)(2,1)S(1)} %collective-permute-done.16.rest_5_), channel_id=1, source_target_pairs={{0,8},{8,0},{16,24},{24,16},{1,9},{9,1},{17,25},{25,17},{2,10},{10... | collective-permute-start | bytes 786440 | tf_op jit(solution)/shard_map/ppermute | solution.py:158
  (38 other events, 509.0 us)
